TPU v7x, 32 devices: a whole 2x2x4 slice. The times are simulated.
32 devices in a mesh: ep: 8 (over z, y), tp: 4 (over x, core).
Axes of the slice: x: 2, y: 2, z: 4, core: 2. Of those that a mesh axis runs over, the one named last changes fastest.
Arguments:
- hidden_in: bfloat16 [128, 1024], P('ep'), may hold values from -6 to 6
- prior_state: float32 [128, 8, 128, 128], P('ep', 'tp'), may hold values from -4 to 4
- mix_gain: float32 [1024], replicated, may hold values from 0.1 to 1.9
- query_w: bfloat16 [1024, 1024], P(None, 'tp'), may hold values from -0.1875 to 0.1875
- key_w: bfloat16 [1024, 1024], P(None, 'tp'), may hold values from -0.1875 to 0.1875
- value_w: bfloat16 [1024, 1024], P(None, 'tp'), may hold values from -0.1875 to 0.1875
- decay_w: bfloat16 [1024, 8], P(None, 'tp'), may hold values from -0.1875 to 0.1875
- beta_w: bfloat16 [1024, 8], P(None, 'tp'), may hold values from -0.1875 to 0.1875
- decay_rate: float32 [8], P('tp'), may hold values from 0.05 to 3
- head_gain: float32 [128], replicated, may hold values from 0.1 to 1.9
- out_w: bfloat16 [1024, 1024], P('tp'), may hold values from -0.1875 to 0.1875
- ffn_gain: float32 [1024], replicated, may hold values from 0.1 to 1.9
- expert_ids: int32 [128, 2], P('ep'), may hold values from 0 to 7, all different within a row; in each aligned block of 16 rows (0 to 15, 16 to 31, ...) at most 10 rows name the same one
- group_share: float32 [128], P('ep'), may hold values from 0.3 to 1
- expert_share: float32 [128, 2], P('ep'), may hold values from 0.1 to 1
- expert_gate: bfloat16 [8, 1024, 512], P('ep', None, 'tp'), may hold values from -0.1875 to 0.1875
- expert_up: bfloat16 [8, 1024, 512], P('ep', None, 'tp'), may hold values from -0.1875 to 0.1875
- expert_down: bfloat16 [8, 512, 1024], P('ep', 'tp'), may hold values from -0.25 to 0.25
- dense_gate: bfloat16 [4096, 1024], P('ep', 'tp'), may hold values from -0.1875 to 0.1875
- dense_up: bfloat16 [4096, 1024], P('ep', 'tp'), may hold values from -0.1875 to 0.1875
- dense_down: bfloat16 [4096, 1024], P('ep', 'tp'), may hold values from -0.25 to 0.25
- branch_gate: bfloat16 [1024], replicated, may hold values from -0.1875 to 0.1875
Outputs:
- layer_out: bfloat16 [128, 1024], P('ep', 'tp')
Inputs may be any that keep to these rules, and one draw needn't show every extreme that they name: `expert_ids`: each row names 2 different experts. Among the rows of one device, no expert is named by more than 10 rows, and in every draw some expert is named by exactly 10 rows of some device.
All inputs are finite; a program needn't handle non-finite values.
Results may differ from a plain program's by a relative error of at most 0.02.
Values may be sent and summed in bfloat16 or wider, within the bound.
A program may use at most 64 MiB of HBM per device.

v0:
```python
import jax
import jax.numpy as jnp
from jax import lax
from jax.sharding import PartitionSpec as P


def rms_scale(values, gain, floor):
    return values * lax.rsqrt(jnp.mean(values * values, axis=-1, keepdims=True) + floor) * gain


def unit_rows(values):
    return values * lax.rsqrt(jnp.sum(values * values, axis=-1, keepdims=True) + 1.0)


def delta_read(queries, key_rows, value_rows, beta_vals, decay_vals, prior_state):
    stacked = jnp.stack([queries, key_rows], axis=2)
    readout = jnp.einsum("shcd,shde->shce", stacked, prior_state, precision=lax.Precision.HIGHEST)
    intersection = jnp.sum(queries * key_rows, axis=-1) * beta_vals
    return decay_vals[..., None] * readout[:, :, 0] + intersection[..., None] * (
        value_rows - decay_vals[..., None] * readout[:, :, 1]
    )


def expert_rows(row_block, w_gate, w_up, w_down):
    gate_pre = jnp.dot(row_block, w_gate, preferred_element_type=jnp.float32)
    up_pre = jnp.dot(row_block, w_up, preferred_element_type=jnp.float32)
    hidden = (jax.nn.silu(gate_pre) * up_pre).astype(jnp.bfloat16)
    partial_out = jnp.dot(hidden, w_down, preferred_element_type=jnp.float32)
    return lax.psum_scatter(
        partial_out.astype(jnp.bfloat16), "tp", scatter_dimension=1, tiled=True
    ).astype(jnp.float32)


def branch_terms(row_block, w_gate, w_up):
    contract = (((1,), (1,)), ((), ()))
    gate_pre = lax.dot_general(w_gate, row_block, contract, preferred_element_type=jnp.float32)
    up_pre = lax.dot_general(w_up, row_block, contract, preferred_element_type=jnp.float32)
    return jnp.stack([gate_pre, up_pre])


def whole_hidden(row_block, w_gate, w_up):
    terms = branch_terms(row_block, w_gate, w_up)
    return (jax.nn.silu(terms[0]) * terms[1]).astype(jnp.bfloat16)


def branch_project(hidden_cols, w_down):
    return lax.dot_general(
        hidden_cols, w_down, (((0,), (0,)), ((), ())), preferred_element_type=jnp.float32
    )


def local(
    hidden_in,
    prior_state,
    mix_gain,
    query_w,
    key_w,
    value_w,
    decay_w,
    beta_w,
    decay_rate,
    head_gain,
    out_w,
    ffn_gain,
    expert_ids,
    group_share,
    expert_share,
    expert_gate,
    expert_up,
    expert_down,
    dense_gate,
    dense_up,
    dense_down,
    branch_gate,
):
    seq_dev, model_width = hidden_in.shape
    heads_local = prior_state.shape[1]
    key_size = prior_state.shape[2]
    value_size = prior_state.shape[3]
    topk_count = expert_ids.shape[1]
    n_ep = lax.axis_size("ep")
    quarter = model_width // lax.axis_size("tp")
    offset = lax.axis_index("tp") * quarter
    capacity = min(seq_dev, 2 * seq_dev * topk_count // n_ep + 2)
    slot_total = n_ep * capacity
    gate_whole, up_whole = (
        lax.all_gather(dense_gate, "tp", axis=1, tiled=True),
        lax.all_gather(dense_up, "tp", axis=1, tiled=True),
    )
    normed = rms_scale(hidden_in.astype(jnp.float32), mix_gain, 0.1).astype(jnp.bfloat16)
    queries = unit_rows(
        jnp.dot(normed, query_w, preferred_element_type=jnp.float32).reshape(
            seq_dev, heads_local, key_size
        )
    )
    key_rows = unit_rows(
        jnp.dot(normed, key_w, preferred_element_type=jnp.float32).reshape(
            seq_dev, heads_local, key_size
        )
    )
    value_rows = jnp.dot(normed, value_w, preferred_element_type=jnp.float32).reshape(
        seq_dev, heads_local, value_size
    )
    beta_vals = jax.nn.sigmoid(jnp.dot(normed, beta_w, preferred_element_type=jnp.float32))
    decay_vals = jnp.exp(
        -decay_rate * jax.nn.softplus(jnp.dot(normed, decay_w, preferred_element_type=jnp.float32))
    )
    readout = delta_read(queries, key_rows, value_rows, beta_vals, decay_vals, prior_state)
    head_out = (
        rms_scale(readout, head_gain, 0.01)
        .astype(jnp.bfloat16)
        .reshape(seq_dev, heads_local * value_size)
    )
    partial_out = jnp.dot(head_out, out_w, preferred_element_type=jnp.float32).astype(jnp.bfloat16)
    mix = lax.psum(partial_out, "tp").astype(jnp.float32)
    resid = (hidden_in.astype(jnp.float32) + mix).astype(jnp.bfloat16)
    normed2 = rms_scale(resid.astype(jnp.float32), ffn_gain, 0.1).astype(jnp.bfloat16)
    resid_own = lax.dynamic_slice_in_dim(resid, offset, quarter, 1).astype(jnp.float32)
    route_weight = (
        group_share[:, None] * expert_share / jnp.sum(expert_share, axis=1, keepdims=True)
    )
    flat_ids = expert_ids.reshape(-1)
    onehot_ids = (flat_ids[:, None] == jnp.arange(n_ep)[None, :]).astype(jnp.int32)
    slot_rank = jnp.sum((jnp.cumsum(onehot_ids, axis=0) - 1) * onehot_ids, axis=1)
    slot_ids = (flat_ids * capacity + slot_rank).reshape(seq_dev, topk_count)
    placing = jnp.sum(
        (slot_ids[:, :, None] == jnp.arange(slot_total)[None, None, :]).astype(jnp.bfloat16), axis=1
    )
    send_rows = lax.dot_general(
        placing, normed2, (((0,), (0,)), ((), ())), preferred_element_type=jnp.float32
    )
    send_rows = send_rows.astype(jnp.bfloat16).reshape(n_ep, capacity, model_width)
    received = lax.all_to_all(send_rows, "ep", split_axis=0, concat_axis=0, tiled=True)
    item_count = received.shape[1]
    flat_rows = received.reshape(n_ep * item_count, model_width)
    summed = expert_rows(flat_rows, expert_gate[0], expert_up[0], expert_down[0])
    back_rows = summed.astype(jnp.bfloat16).reshape(n_ep, item_count, quarter)
    returned = lax.all_to_all(back_rows, "ep", split_axis=0, concat_axis=0, tiled=True)
    picked = returned.reshape(slot_total, quarter)[slot_ids]
    moe = jnp.sum(picked.astype(jnp.float32) * route_weight[:, :, None], axis=1)
    hidden = whole_hidden(lax.all_gather(normed2, "ep", axis=0, tiled=True), gate_whole, up_whole)
    branch_own = lax.psum_scatter(
        branch_project(hidden, dense_down), "ep", scatter_dimension=0, tiled=True
    )
    branch_weight = jax.nn.sigmoid(
        jnp.dot(normed2, branch_gate, preferred_element_type=jnp.float32)
    )
    result = resid_own + moe + branch_weight[:, None] * branch_own
    return result.astype(jnp.bfloat16)


def solution(mesh):
    placed = (
        P("ep", None),
        P("ep", "tp", None, None),
        P(),
        P(None, "tp"),
        P(None, "tp"),
        P(None, "tp"),
        P(None, "tp"),
        P(None, "tp"),
        P("tp"),
        P(),
        P("tp", None),
        P(),
        P("ep", None),
        P("ep"),
        P("ep", None),
        P("ep", None, "tp"),
        P("ep", None, "tp"),
        P("ep", "tp", None),
        P("ep", "tp"),
        P("ep", "tp"),
        P("ep", "tp"),
        P(),
    )
    return jax.shard_map(
        local, mesh=mesh, in_specs=placed, out_specs=P("ep", "tp"), check_vma=False
    )
```

profile of v0, /device:TPU:0, one launch (start us, length us, event | category | flops | bytes accessed | tf_op | source)
XLA Modules:
  0.0 164.1 jit_solution(9147317888466888396)
XLA Ops:
  6.5 0.7 all-gather.3.cloned.1.call-update
  7.3 0.7 all-gather.5.cloned.1.call-update
  8.1 0.9 fusion.26
  8.9 1.3 fusion.60
  10.3 1.3 fusion.58
  11.9 0.2 multiply_reduce_fusion.2
  12.1 0.1 broadcast_multiply_fusion
  12.3 1.9 %fusion.35 = f32[16,2,2,128]{3,2,1,0:T(2,128)S(1)} fusion(f32[16,2,128,128]{3,2,1,0:T(8,128)S(1)} %copy-done, f32[16,2,1,128]{3,2,1,0:T(1,128)S(1)} %get-tuple-element.12, f32[16,2,1,128]{3,2,1,0:T(1,128)S(1)} %get-tuple-element.13), kind=kOutput, calls=%fused_computation.48 | convolution fusion | flops 12591104 | bytes 2162688 | tf_op jit(solution)/shard_map/shcd,shde->shce/dot_general | solution.py:17
  14.3 0.2 fusion.7
  14.6 0.2 fusion.55
  14.9 0.2 fusion.51
  15.2 0.2 multiply_reduce_fusion.1
  15.7 0.2 convolution_convert_fusion.2
  15.9 13.6 %psum.7 = bf16[16,1024]{1,0:T(8,128)(2,1)S(1)} all-reduce(bf16[16,1024]{1,0:T(8,128)(2,1)S(1)} %convolution_convert_fusion.2), channel_id=1, replica_groups=mesh['ep'=8,'tp'=4] {'tp'}, use_global_device_ids=true, to_apply=%region_5.6 | all-reduce | flops 16384 | bytes 65536 | tf_op jit(solution)/shard_map/psum | solution.py:115
  29.4 0.1 fusion.23
  29.9 0.2 select_reduce_fusion
  30.4 0.2 convolution_convert_fusion.1
  30.6 0.8 reshape.114
  31.4 5.8 %all-to-all-start = ((bf16[8,10,1024]{2,1,0:T(8,128)(2,1)}), bf16[8,10,1024]{2,1,0:T(8,128)(2,1)S(1)}, u32[]{:S(2)}, u32[]{:S(2)}) async-start(bf16[8,10,1024]{2,1,0:T(8,128)(2,1)} %reshape.114), calls=%async_computation | async-start | bytes 524288 | tf_op jit(solution)/shard_map/all_to_all | solution.py:133
  37.3 32.3 %all_gather.9 = bf16[128,1024]{1,0:T(8,128)(2,1)S(1)} all-gather(bf16[16,1024]{1,0:T(8,128)(2,1)S(1)} %fusion.25), channel_id=1, replica_groups=mesh['ep'=8,'tp'=4] {'ep'}, dimensions={0}, use_global_device_ids=true | all-gather | bytes 294912 | tf_op jit(solution)/shard_map/all_gather | solution.py:141
  69.6 0.1 fusion.11
  69.8 1.1 fusion.15
  71.0 1.0 convolution_convert_fusion
  72.1 1.7 %convolution_bitcast_fusion.1 = f32[512,128]{0,1:T(8,128)S(1)} fusion(bf16[128,1024]{1,0:T(8,128)(2,1)S(1)} %all_gather.9, bf16[512,1024]{1,0:T(8,128)(2,1)} %all-gather.3.cloned.1.call-done), kind=kOutput, calls=%fused_computation.2 | convolution fusion | flops 134217728 | bytes 1572864 | tf_op jit(solution)/shard_map/dot_general | solution.py:36
  73.9 2.5 %fusion.2 = f32[128,256]{1,0:T(8,128)} fusion(bf16[512,256]{1,0:T(8,128)(2,1)} %param.42, bf16[128,1024]{1,0:T(8,128)(2,1)S(1)} %all_gather.9, bf16[512,1024]{1,0:T(8,128)(2,1)} %all-gather.5.cloned.1.call-done, f32[512,128]{0,1:T(8,128)S(1)} %convolution_bitcast_fusion.1), kind=kOutput, calls=%fused_computation.7 | convolution fusion | flops 168165376 | bytes 1966080 | tf_op jit(solution)/shard_map/dot_general | solution.py:47
  76.7 14.3 %reduce-scatter.3.cloned.1.call-done = bf16[80,256]{1,0:T(8,128)(2,1)} async-done(((bf16[80,1024]{1,0:T(8,128)(2,1)}), bf16[80,256]{1,0:T(8,128)(2,1)}) %reduce-scatter.3.cloned.1.call-update) | async-done | bytes 40976 | tf_op jit(solution)/shard_map/reduce_scatter | solution.py:29
  91.0 1.4 reshape.116
  92.5 5.5 %all-to-all-start.1 = ((bf16[8,10,256]{2,1,0:T(8,128)(2,1)}), bf16[8,10,256]{2,1,0:T(8,128)(2,1)S(1)}, u32[]{:S(2)}, u32[]{:S(2)}) async-start(bf16[8,10,256]{2,1,0:T(8,128)(2,1)} %reshape.116), calls=%async_computation.2 | async-start | bytes 131072 | tf_op jit(solution)/shard_map/all_to_all | solution.py:138
  98.0 6.9 %all-to-all-done.1 = bf16[8,10,256]{2,1,0:T(8,128)(2,1)S(1)} async-done(((bf16[8,10,256]{2,1,0:T(8,128)(2,1)}), bf16[8,10,256]{2,1,0:T(8,128)(2,1)S(1)}, u32[]{:S(2)}, u32[]{:S(2)}) %all-to-all-start.1) | async-done | bytes 40992 | tf_op jit(solution)/shard_map/all_to_all | solution.py:138
  104.9 0.6 gather_fusion
  105.7 50.5 %reduce-scatter.5.cloned.1.call-done = f32[16,256]{1,0:T(8,128)} async-done(((f32[128,256]{1,0:T(8,128)}), f32[16,256]{1,0:T(8,128)}) %reduce-scatter.5.cloned.1.call-update) | async-done | bytes 16400 | tf_op jit(solution)/shard_map/reduce_scatter | solution.py:142
  156.2 1.4 add_convert_fusion
  (82 shorter events, 2.3 us)
Async XLA Ops:
  6.5 5.7 %copy-start = (f32[16,2,128,128]{3,2,1,0:T(8,128)S(1)}, f32[16,2,128,128]{3,2,1,0:T(8,128)}, u32[]{:S(2)}) copy-start(f32[16,2,128,128]{3,2,1,0:T(8,128)} %param.23) | copy-start | bytes 6291460
  6.5 65.6 %all-gather.3.cloned.1.call-start = ((), (), s32[]{:S(2)}) async-start(), calls=%async_computation.5 | async-start | bytes 1310720 | tf_op jit(solution)/shard_map/all_gather | solution.py:87
  7.3 7.0 %copy-start.1 = (bf16[16,1024]{1,0:T(8,128)(2,1)S(1)}, bf16[16,1024]{1,0:T(8,128)(2,1)}, u32[]{:S(2)}) copy-start(bf16[16,1024]{1,0:T(8,128)(2,1)} %param.22) | copy-start | bytes 98308
  7.3 7.0 %copy-start.6 = (f32[1024]{0:T(1024)S(1)}, f32[1024]{0:T(1024)}, u32[]{:S(2)}) copy-start(f32[1024]{0:T(1024)} %param.24) | copy-start | bytes 12292
  7.3 7.0 %copy-start.12 = (bf16[1024,2]{0,1:T(2,128)(2,1)S(1)}, bf16[1024,2]{0,1:T(2,128)(2,1)}, u32[]{:S(2)}) copy-start(bf16[1024,2]{0,1:T(2,128)(2,1)} %param.29) | copy-start | bytes 12292
  7.3 7.3 %copy-start.3 = (bf16[1024,256]{1,0:T(8,128)(2,1)S(1)}, bf16[1024,256]{1,0:T(8,128)(2,1)}, u32[]{:S(2)}) copy-start(bf16[1024,256]{1,0:T(8,128)(2,1)} %param.27) | copy-start | bytes 1572868
  7.3 66.6 %all-gather.5.cloned.1.call-start = ((), (), s32[]{:S(2)}) async-start(), calls=%async_computation.6 | async-start | bytes 1310720 | tf_op jit(solution)/shard_map/all_gather | solution.py:88
  10.2 4.6 %copy-start.14 = (f32[2]{0:T(128)S(1)}, f32[2]{0:T(128)}, u32[]{:S(2)}) copy-start(f32[2]{0:T(128)} %param.30) | copy-start | bytes 28
  10.2 4.6 %copy-start.13 = (bf16[1024,2]{0,1:T(2,128)(2,1)S(1)}, bf16[1024,2]{0,1:T(2,128)(2,1)}, u32[]{:S(2)}) copy-start(bf16[1024,2]{0,1:T(2,128)(2,1)} %param.28) | copy-start | bytes 12292
  10.2 5.2 %copy-start.15 = (f32[128]{0:T(128)S(1)}, f32[128]{0:T(128)}, u32[]{:S(2)}) copy-start(f32[128]{0:T(128)} %param.31) | copy-start | bytes 1540
  10.3 5.4 %copy-start.2 = (bf16[256,1024]{1,0:T(8,128)(2,1)S(1)}, bf16[256,1024]{1,0:T(8,128)(2,1)}, u32[]{:S(2)}) copy-start(bf16[256,1024]{1,0:T(8,128)(2,1)} %param.32) | copy-start | bytes 1572868
  12.1 17.4 %copy-start.9 = (s32[16,2]{0,1:T(2,128)S(1)}, s32[16,2]{0,1:T(2,128)}, u32[]{:S(2)}) copy-start(s32[16,2]{0,1:T(2,128)} %param.34) | copy-start | bytes 388
  12.3 18.1 %copy-start.7 = (f32[1024]{0:T(1024)S(1)}, f32[1024]{0:T(1024)}, u32[]{:S(2)}) copy-start(f32[1024]{0:T(1024)} %param.33) | copy-start | bytes 12292
  14.1 23.1 %copy-start.10 = (bf16[1024]{0:T(1024)(128)(2,1)S(1)}, bf16[1024]{0:T(1024)(128)(2,1)}, u32[]{:S(2)}) copy-start(bf16[1024]{0:T(1024)(128)(2,1)} %param.43) | copy-start | bytes 6148
  14.1 23.1 %copy-start.8 = (f32[16,2]{0,1:T(2,128)S(1)}, f32[16,2]{0,1:T(2,128)}, u32[]{:S(2)}) copy-start(f32[16,2]{0,1:T(2,128)} %param.36) | copy-start | bytes 388
  14.6 56.4 %copy-start.4 = (bf16[1,128,1024]{2,1,0:T(8,128)(2,1)S(1)}, bf16[1,128,1024]{2,1,0:T(8,128)(2,1)}, u32[]{:S(2)}) copy-start(bf16[1,128,1024]{2,1,0:T(8,128)(2,1)} %param.39) | copy-start | bytes 786436
  14.8 56.1 %copy-start.5 = (bf16[1,1024,128]{2,1,0:T(8,128)(2,1)S(1)}, bf16[1,1024,128]{2,1,0:T(8,128)(2,1)}, u32[]{:S(2)}) copy-start(bf16[1,1024,128]{2,1,0:T(8,128)(2,1)} %param.38) | copy-start | bytes 786436
  31.4 38.3 %all-to-all-start = ((bf16[8,10,1024]{2,1,0:T(8,128)(2,1)}), bf16[8,10,1024]{2,1,0:T(8,128)(2,1)S(1)}, u32[]{:S(2)}, u32[]{:S(2)}) async-start(bf16[8,10,1024]{2,1,0:T(8,128)(2,1)} %reshape.114), calls=%async_computation | async-start | bytes 524288 | tf_op jit(solution)/shard_map/all_to_all | solution.py:133
  37.2 53.8 %reduce-scatter.3.cloned.1.call-start = ((), (), s32[]{:S(2)}) async-start(), calls=%async_computation.4 | async-start | bytes 204800 | tf_op jit(solution)/shard_map/reduce_scatter | solution.py:29
  72.0 4.4 %copy-start.11 = (f32[16]{0:T(128)S(1)}, f32[16]{0:T(128)}, u32[]{:S(2)}) copy-start(f32[16]{0:T(128)} %param.35) | copy-start | bytes 196
  72.0 84.1 %reduce-scatter.5.cloned.1.call-start = ((), (), s32[]{:S(2)}) async-start(), calls=%async_computation.7 | async-start | bytes 147456 | tf_op jit(solution)/shard_map/reduce_scatter | solution.py:142
  92.5 12.4 %all-to-all-start.1 = ((bf16[8,10,256]{2,1,0:T(8,128)(2,1)}), bf16[8,10,256]{2,1,0:T(8,128)(2,1)S(1)}, u32[]{:S(2)}, u32[]{:S(2)}) async-start(bf16[8,10,256]{2,1,0:T(8,128)(2,1)} %reshape.116), calls=%async_computation.2 | async-start | bytes 131072 | tf_op jit(solution)/shard_map/all_to_all | solution.py:138
Sparse Core Ops, SparseCore 0:
  8.9 19.9 all-gather.2
  30.5 16.7 all-gather.4
  72.2 18.8 reduce-scatter.2
  94.2 61.9 reduce-scatter.4
where the time goes:
time: 165 us; the launch traced here: 164 us
  waiting for transfers between devices  73.2 us (44%)
  blocking collectives  45.9 us (28%)
  between operations  13.5 us (8%)
  matrix products  12.1 us (7%)
  starting transfers between devices  11.4 us (7%)
  local copies, waits for them, and re-layouts  4.28 us (3%)
  other arithmetic  3.75 us (2%)
    reduce_scatter x1, waiting for transfers between devices, local(): lax.psum_scatter(branch_project(hidden, dense_down), 'ep', scatter_dimens...  50.5 us
    all_gather x1, blocking collectives, local(): lax.all_gather(normed2, 'ep', axis=0, tiled=True)  32.3 us
    reduce_scatter x1, waiting for transfers between devices, expert_rows(): lax.psum_scatter(partial_out.astype(jnp.bfloat16), 'tp', scatter_dimensio...  14.3 us
    psum x1, blocking collectives, local(): mix = lax.psum(partial_out, 'tp').astype(jnp.float32)  13.6 us
    all_to_all x1, waiting for transfers between devices, local(): lax.all_to_all(back_rows, 'ep', split_axis=0, concat_axis=0, tiled=True)  6.9 us
    all_to_all x1, starting transfers between devices, local(): lax.all_to_all(send_rows, 'ep', split_axis=0, concat_axis=0, tiled=True)  5.79 us
    all_to_all x1, starting transfers between devices, local(): lax.all_to_all(back_rows, 'ep', split_axis=0, concat_axis=0, tiled=True)  5.53 us
  transfers between devices with their start and end apart: 6, of which 3 were waited for; matrix products, arithmetic and copies ran while one was open for 11% of the time, Pallas kernels for 0%

commit v1 on v0

v1 whole, which is shorter than its diff:
```python
import functools

import jax
import jax.numpy as jnp
from jax import lax
from jax.experimental import pallas as pl
from jax.experimental.pallas import tpu as pltpu
from jax.sharding import PartitionSpec as P

MESH = pl.DeviceIdType.MESH
NT = (((1,), (1,)), ((), ()))


def rms_scale(values, gain, floor):
    return values * lax.rsqrt(jnp.mean(values * values, axis=-1, keepdims=True) + floor) * gain


def unit_rows(values):
    return values * lax.rsqrt(jnp.sum(values * values, axis=-1, keepdims=True) + 1.0)


def mm(lhs, rhs):
    return jnp.dot(lhs, rhs, preferred_element_type=jnp.float32)


def each(low, high, body):
    if high - low <= 16:
        for step in range(low, high):
            body(step)
    else:

        def looped(step, carry):
            body(step)
            return carry

        lax.fori_loop(low, high, looped, 0)


def kernel(
    n_ep,
    n_tp,
    hidden_ref,
    mix_gain_ref,
    decay_w_ref,
    beta_w_ref,
    decay_rate_ref,
    head_gain_ref,
    ffn_gain_ref,
    ids_ref,
    group_ref,
    share_ref,
    branch_gate_ref,
    state_hbm,
    query_hbm,
    key_hbm,
    value_hbm,
    out_w_hbm,
    egate_hbm,
    eup_hbm,
    edown_hbm,
    dgate_hbm,
    dup_hbm,
    ddown_hbm,
    out_ref,
    state_v,
    qkv_v,
    out_w_v,
    egu_v,
    edown_v,
    ddown_v,
    wide,
    part,
    resid_v,
    rows,
    esend,
    erecv,
    fsend,
    frecv,
    local_sem,
    wide_send,
    wide_recv,
    part_send,
    part_recv,
    rows_send,
    rows_recv,
    e_send,
    e_recv,
    f_send,
    f_recv,
):
    me_e = lax.axis_index("ep")
    me_t = lax.axis_index("tp")
    seq, width = hidden_ref.shape
    heads = state_v.shape[1]
    key_size = state_v.shape[2]
    quarter = out_ref.shape[1]

    def partner(bit):
        return me_t + bit - 2 * bit * ((me_t // bit) % 2)

    loads = []

    def load(src, dst):
        copy = pltpu.make_async_copy(src, dst, local_sem.at[len(loads)])
        copy.start()
        loads.append(copy)
        return copy

    qkv_loads = [
        load(query_hbm, qkv_v.at[0]),
        load(key_hbm, qkv_v.at[1]),
        load(value_hbm, qkv_v.at[2]),
    ]
    cut = 4 if seq % 4 == 0 else 1
    step_rows = seq // cut
    state_loads = [
        load(
            state_hbm.at[pl.ds(i * step_rows, step_rows)],
            state_v.at[pl.ds(i * step_rows, step_rows)],
        )
        for i in range(cut)
    ]
    out_load = load(out_w_hbm, out_w_v)
    barrier = pltpu.get_barrier_semaphore()

    def greet_ep(step):
        pl.semaphore_signal(
            barrier, inc=1, device_id={"ep": (me_e + step) % n_ep}, device_id_type=MESH
        )

    def greet_tp(step):
        pl.semaphore_signal(
            barrier, inc=1, device_id={"tp": (me_t + step) % n_tp}, device_id_type=MESH
        )

    each(1, n_tp, greet_tp)
    each(1, n_ep, greet_ep)
    wide_loads = [load(dgate_hbm, wide.at[0, me_t]), load(dup_hbm, wide.at[1, me_t])]
    moe_loads = [
        load(egate_hbm.at[0], egu_v.at[0]),
        load(eup_hbm.at[0], egu_v.at[1]),
        load(edown_hbm.at[0], edown_v),
    ]
    down_load = load(ddown_hbm, ddown_v)
    pl.semaphore_wait(barrier, n_ep + n_tp - 2)

    bits = []
    bit = n_tp // 2
    while bit >= 1:
        bits.append(bit)
        bit //= 2

    def wide_copy(which, src, slot, bit, index):
        return pltpu.make_async_remote_copy(
            src_ref=src,
            dst_ref=wide.at[which, slot],
            send_sem=wide_send.at[which, index],
            recv_sem=wide_recv.at[which, index],
            device_id={"tp": partner(bit)},
            device_id_type=MESH,
        )

    wide_all = ({}, {})

    def send_own(which):
        src = (dgate_hbm, dup_hbm)[which]
        for bit in bits:
            copy = wide_copy(which, src, me_t, bit, bit)
            copy.start()
            wide_all[which][bit] = copy

    def flip(value, bit):
        return value + bit - 2 * bit * ((value // bit) % 2)

    def relay(which):
        arrived = []
        for at, bit in enumerate(bits):
            fresh = [bit] + [mask + bit for mask in arrived]
            arrived = arrived + fresh
            for mask in fresh:
                if at < len(bits) - 1:
                    wide_all[which][mask].wait_recv()
                    slot = me_t
                    for one in bits:
                        if mask & one:
                            slot = flip(slot, one)
                    for lower in bits[at + 1 :]:
                        copy = wide_copy(which, wide.at[which, slot], slot, lower, mask + lower)
                        copy.start()
                        wide_all[which][mask + lower] = copy

    send_own(0)

    hidden = hidden_ref[...].astype(jnp.float32)
    normed = rms_scale(hidden, mix_gain_ref[...], 0.1).astype(jnp.bfloat16)
    beta = jax.nn.sigmoid(mm(normed, beta_w_ref[...]))
    decay_pre = mm(normed, decay_w_ref[...])
    softplus = jnp.maximum(decay_pre, 0.0) + jnp.log1p(jnp.exp(-jnp.abs(decay_pre)))
    group_row = group_ref[...]
    diagonal = lax.broadcasted_iota(jnp.int32, (seq, seq), 0) == lax.broadcasted_iota(
        jnp.int32, (seq, seq), 1
    )
    group_col = jnp.sum(
        jnp.where(diagonal, jnp.broadcast_to(group_row, (seq, seq)), 0.0), axis=1, keepdims=True
    )
    share = share_ref[...]
    ids = ids_ref[...]
    route = group_col * share / jnp.sum(share, axis=1, keepdims=True)
    pad = rows.shape[2] - width
    lanes = lax.broadcasted_iota(jnp.int32, (seq, pad), 1)
    spread = jnp.zeros((seq, pad), jnp.float32)
    for k in range(ids.shape[1]):
        spread = spread + jnp.where(ids[:, k : k + 1] == lanes, route[:, k : k + 1], 0.0)

    for copy in qkv_loads:
        copy.wait()
    queries = mm(normed, qkv_v[0])
    keys = mm(normed, qkv_v[1])
    values = mm(normed, qkv_v[2])
    row_of = lax.broadcasted_iota(jnp.int32, (seq, out_w_v.shape[0] // heads), 0)
    q_rows, k_rows, stacked = [], [], []
    for h in range(heads):
        span = slice(h * key_size, (h + 1) * key_size)
        q_rows.append(unit_rows(queries[:, span]))
        k_rows.append(unit_rows(keys[:, span]))
        stacked.append(jnp.concatenate([q_rows[h], k_rows[h]], axis=0).astype(jnp.bfloat16))
    read_q = [jnp.zeros(row_of.shape, jnp.float32) for _ in range(heads)]
    read_k = [jnp.zeros(row_of.shape, jnp.float32) for _ in range(heads)]
    for s in range(seq):
        if s % step_rows == 0:
            state_loads[s // step_rows].wait()
        for h in range(heads):
            both = mm(stacked[h], state_v[s, h].astype(jnp.bfloat16))
            read_q[h] = jnp.where(row_of == s, both[:seq], read_q[h])
            read_k[h] = jnp.where(row_of == s, both[seq:], read_k[h])
    outs = []
    value_size = row_of.shape[1]
    for h in range(heads):
        decay = jnp.exp(-decay_rate_ref[h] * softplus[:, h : h + 1])
        inner = jnp.sum(q_rows[h] * k_rows[h], axis=1, keepdims=True) * beta[:, h : h + 1]
        value_rows = values[:, h * value_size : (h + 1) * value_size]
        readout = decay * read_q[h] + inner * (value_rows - decay * read_k[h])
        outs.append(rms_scale(readout, head_gain_ref[...], 0.01).astype(jnp.bfloat16))
    out_load.wait()
    part[me_t] = mm(jnp.concatenate(outs, axis=1), out_w_v[...]).astype(jnp.bfloat16)
    part_copies = []
    for step in range(1, n_tp):
        copy = pltpu.make_async_remote_copy(
            src_ref=part.at[me_t],
            dst_ref=part.at[me_t],
            send_sem=part_send.at[step],
            recv_sem=part_recv.at[step],
            device_id={"tp": (me_t + step) % n_tp},
            device_id_type=MESH,
        )
        copy.start()
        part_copies.append(copy)
    send_own(1)
    for copy in part_copies:
        copy.wait_recv()
    mix = part[0].astype(jnp.float32)
    for t in range(1, n_tp):
        mix = mix + part[t].astype(jnp.float32)
    resid = (hidden + mix).astype(jnp.bfloat16).astype(jnp.float32)
    resid_v[...] = resid
    rows[me_e, :, :width] = rms_scale(resid, ffn_gain_ref[...], 0.1).astype(jnp.bfloat16)
    rows[me_e, :, width:] = spread.astype(jnp.bfloat16)

    def send_rows(step):
        pltpu.make_async_remote_copy(
            src_ref=rows.at[me_e],
            dst_ref=rows.at[me_e],
            send_sem=rows_send,
            recv_sem=rows_recv,
            device_id={"ep": (me_e + step) % n_ep},
            device_id_type=MESH,
        ).start()

    each(1, n_ep, send_rows)
    relay(0)
    for copy in moe_loads:
        copy.wait()

    def wait_bytes(ref, sem):
        pltpu.make_async_copy(ref, ref, sem).wait()

    wait_bytes(rows.at[pl.ds(0, n_ep - 1)], rows_recv)

    group = min(n_ep, 8)
    tall = group * seq

    def expert_block(block):
        both = rows[pl.ds(block * group, group)].reshape(tall, rows.shape[2])
        row_block = both[:, :width]
        weights = both[:, width:].astype(jnp.float32)
        mine = lax.broadcasted_iota(jnp.int32, weights.shape, 1) == me_e
        weight = jnp.sum(jnp.where(mine, weights, 0.0), axis=1, keepdims=True)
        gate = mm(row_block, egu_v[0])
        up = mm(row_block, egu_v[1])
        unit = (gate * jax.nn.sigmoid(gate) * up).astype(jnp.bfloat16)
        outs = mm(unit, edown_v[...]) * weight
        for t in range(n_tp):
            esend[t, pl.ds(block * tall, tall)] = outs[:, t * quarter : (t + 1) * quarter].astype(
                jnp.bfloat16
            )

    each(0, n_ep // group, expert_block)
    e_copies = []
    for step in range(1, n_tp):
        peer = (me_t + step) % n_tp
        copy = pltpu.make_async_remote_copy(
            src_ref=esend.at[peer],
            dst_ref=erecv.at[step - 1],
            send_sem=e_send.at[step],
            recv_sem=e_recv.at[step],
            device_id={"tp": peer},
            device_id_type=MESH,
        )
        copy.start()
        e_copies.append(copy)
    relay(1)
    for copy in wide_loads:
        copy.wait()
    down_load.wait()
    last = [mask for mask in range(1, n_tp) if mask % 2 == 1]
    for which in (0, 1):
        for mask in last:
            wide_all[which][mask].wait_recv()

    def branch_block(block):
        at = pl.ds(block * tall, tall)
        row_block = rows[pl.ds(block * group, group)].reshape(tall, rows.shape[2])[:, :width]
        gate, up = 0.0, 0.0
        for t in range(n_tp):
            piece = row_block[:, t * quarter : (t + 1) * quarter]
            gate = gate + lax.dot_general(
                piece, wide[0, t], NT, preferred_element_type=jnp.float32
            )
            up = up + lax.dot_general(piece, wide[1, t], NT, preferred_element_type=jnp.float32)
        unit = (gate * jax.nn.sigmoid(gate) * up).astype(jnp.bfloat16)
        branch = mm(unit, ddown_v[...])
        pre = jnp.sum(
            row_block.astype(jnp.float32) * branch_gate_ref[...].astype(jnp.float32),
            axis=1,
            keepdims=True,
        )
        return jax.nn.sigmoid(pre) * branch + esend[me_t, at].astype(jnp.float32)

    def store_block(block, total):
        fsend[pl.ds(block * group, group)] = total.astype(jnp.bfloat16).reshape(
            group, seq, quarter
        )

    def finish(block, total):
        at = pl.ds(block * tall, tall)
        for step in range(n_tp - 1):
            total = total + erecv[step, at].astype(jnp.float32)
        store_block(block, total)

    if n_ep == group:
        total = branch_block(0)
        for copy in e_copies:
            copy.wait_recv()
        finish(0, total)
    else:
        for copy in e_copies:
            copy.wait_recv()
        each(0, n_ep // group, lambda block: finish(block, branch_block(block)))

    def send_final(step):
        peer = (me_e + step) % n_ep
        pltpu.make_async_remote_copy(
            src_ref=fsend.at[peer],
            dst_ref=frecv.at[step - 1],
            send_sem=f_send,
            recv_sem=f_recv,
            device_id={"ep": peer},
            device_id_type=MESH,
        ).start()

    each(1, n_ep, send_final)
    mine = pl.ds(pl.multiple_of(me_t * quarter, quarter), quarter)
    total = resid_v[:, mine] + fsend[me_e].astype(jnp.float32)
    wait_bytes(frecv, f_recv)
    total = total + jnp.sum(frecv[...].astype(jnp.float32), axis=0)
    out_ref[...] = total.astype(jnp.bfloat16)
    wait_bytes(frecv, f_send)
    wait_bytes(rows.at[pl.ds(0, n_ep - 1)], rows_send)
    for copy in part_copies + e_copies:
        copy.wait_send()
    for which in (0, 1):
        for copy in wide_all[which].values():
            copy.wait_send()


def local(n_ep, n_tp, *args):
    (
        hidden_in,
        prior_state,
        mix_gain,
        query_w,
        key_w,
        value_w,
        decay_w,
        beta_w,
        decay_rate,
        head_gain,
        out_w,
        ffn_gain,
        expert_ids,
        group_share,
        expert_share,
        expert_gate,
        expert_up,
        expert_down,
        dense_gate,
        dense_up,
        dense_down,
        branch_gate,
    ) = args
    seq, width = hidden_in.shape
    quarter = width // n_tp
    tokens = n_ep * seq
    pad = -(-n_ep // 128) * 128
    vmem = pl.BlockSpec(memory_space=pltpu.VMEM)
    anywhere = pl.BlockSpec(memory_space=pl.ANY)
    bf16 = jnp.bfloat16
    dma = pltpu.SemaphoreType.DMA
    return pl.pallas_call(
        functools.partial(kernel, n_ep, n_tp),
        out_shape=jax.ShapeDtypeStruct((seq, quarter), bf16),
        in_specs=[vmem] * 4
        + [pl.BlockSpec(memory_space=pltpu.SMEM)]
        + [vmem] * 6
        + [anywhere] * 11,
        out_specs=vmem,
        scratch_shapes=[
            pltpu.VMEM(prior_state.shape, jnp.float32),
            pltpu.VMEM((3,) + query_w.shape, bf16),
            pltpu.VMEM(out_w.shape, bf16),
            pltpu.VMEM((2,) + expert_gate.shape[1:], bf16),
            pltpu.VMEM(expert_down.shape[1:], bf16),
            pltpu.VMEM(dense_down.shape, bf16),
            pltpu.VMEM((2, n_tp) + dense_gate.shape, bf16),
            pltpu.VMEM((n_tp, seq, width), bf16),
            pltpu.VMEM((seq, width), jnp.float32),
            pltpu.VMEM((n_ep, seq, width + pad), bf16),
            pltpu.VMEM((n_tp, tokens, quarter), bf16),
            pltpu.VMEM((n_tp - 1, tokens, quarter), bf16),
            pltpu.VMEM((n_ep, seq, quarter), bf16),
            pltpu.VMEM((n_ep - 1, seq, quarter), bf16),
            dma((16,)),
            dma((2, n_tp)),
            dma((2, n_tp)),
            dma((n_tp,)),
            dma((n_tp,)),
            dma,
            dma,
            dma((n_tp,)),
            dma((n_tp,)),
            dma,
            dma,
        ],
        compiler_params=pltpu.CompilerParams(
            collective_id=0, has_side_effects=True, vmem_limit_bytes=56 * 1024 * 1024
        ),
        name="layer_step",
    )(
        hidden_in,
        mix_gain[None, :],
        decay_w,
        beta_w,
        decay_rate,
        head_gain[None, :],
        ffn_gain[None, :],
        expert_ids,
        group_share[None, :],
        expert_share,
        branch_gate[None, :],
        prior_state,
        query_w,
        key_w,
        value_w,
        out_w,
        expert_gate,
        expert_up,
        expert_down,
        dense_gate,
        dense_up,
        dense_down,
    )


def solution(mesh):
    placed = (
        P("ep", None),
        P("ep", "tp", None, None),
        P(),
        P(None, "tp"),
        P(None, "tp"),
        P(None, "tp"),
        P(None, "tp"),
        P(None, "tp"),
        P("tp"),
        P(),
        P("tp", None),
        P(),
        P("ep", None),
        P("ep"),
        P("ep", None),
        P("ep", None, "tp"),
        P("ep", None, "tp"),
        P("ep", "tp", None),
        P("ep", "tp"),
        P("ep", "tp"),
        P("ep", "tp"),
        P(),
    )
    body = functools.partial(local, mesh.shape["ep"], mesh.shape["tp"])
    return jax.shard_map(
        body, mesh=mesh, in_specs=placed, out_specs=P("ep", "tp"), check_vma=False
    )
```

time: 165 us -> 43.8 us (0.27)
  waiting for transfers between devices: 73.2 us -> 0 us
  blocking collectives: 45.9 us -> 0 us
  Pallas kernels: 0 us -> 35 us
  between operations: 13.5 us -> 0.01 us
  matrix products: 12.1 us -> 0 us
  starting transfers between devices: 11.4 us -> 0 us
  local copies, waits for them, and re-layouts: 4.28 us -> 8.39 us
  other arithmetic: 3.75 us -> 0 us
    reduce_scatter x2 -> x0, waiting for transfers between devices: 64.8 us -> none  [the longest x1 50.5 us: local(): lax.psum_scatter(branch_project(hidden, dense_down), 'ep', scatter_dimens...]
    pallas_call x0 -> x1, Pallas kernels: none -> 35 us  [local(): pl.pallas_call(functools.partial(kernel, n_ep, n_tp), out_shape=jax.Shape...]
    all_gather x1 -> x0, blocking collectives: 32.3 us -> none  [local(): lax.all_gather(normed2, 'ep', axis=0, tiled=True)]
    psum x1 -> x0, blocking collectives: 13.6 us -> none  [local(): mix = lax.psum(partial_out, 'tp').astype(jnp.float32)]
    dot_general x13 -> x0, matrix products: 12.1 us -> none  [the longest x1 2.53 us: branch_project(): lax.dot_general(hidden_cols, w_down, (((0,), (0,)), ((), ())), preferred_...]
    all_to_all x2 -> x0, starting transfers between devices: 11.3 us -> none  [the longest x1 5.79 us: local(): lax.all_to_all(send_rows, 'ep', split_axis=0, concat_axis=0, tiled=True)]
    unnamed x34 -> x5, local copies, waits for them, and re-layouts: 0.18 us -> 7.11 us
    all_to_all x2 -> x0, waiting for transfers between devices: 6.91 us -> none  [the longest x1 6.9 us: local(): lax.all_to_all(back_rows, 'ep', split_axis=0, concat_axis=0, tiled=True)]
  transfers between devices with their start and end apart: 6 -> 0, of which waited for: 3 -> 0; matrix products, arithmetic and copies ran while one was open for 11% -> 0% of each run, Pallas kernels for 0% -> 0%
where the time goes in v1:
time: 43.8 us; the launch traced here: 43.4 us
  Pallas kernels  35 us (80%)
  local copies, waits for them, and re-layouts  8.39 us (19%)
    pallas_call x1, Pallas kernels, local(): pl.pallas_call(functools.partial(kernel, n_ep, n_tp), out_shape=jax.Shape...  35 us
    unnamed x5, local copies, waits for them, and re-layouts  7.11 us
    broadcast_in_dim x1, local copies, waits for them, and re-layouts, local(): branch_gate[None, :]  1.28 us

profile of v1, /device:TPU:0, one launch (start us, length us, event | category | flops | bytes accessed | tf_op | source)
XLA Modules:
  0.0 43.4 jit_solution(17050799063019502654)
XLA Ops:
  0.0 1.3 %broadcast_in_dim.19.branch_gate_ref = bf16[1,1024]{1,0:T(2,128)(2,1)} reshape(bf16[1024]{0:T(1024)(128)(2,1)} %param.43) | data formatting | bytes 4096 | tf_op jit(solution)/shard_map/broadcast_in_dim | solution.py:479
  1.3 1.4 %copy.25.ids_ref = s32[16,2]{1,0:T(8,128)} copy(s32[16,2]{0,1:T(2,128)} %param.34) | data formatting | bytes 256 | tf_op args[12]
  2.6 1.3 %copy.26.share_ref = f32[16,2]{1,0:T(8,128)} copy(f32[16,2]{0,1:T(2,128)} %param.36) | data formatting | bytes 256 | tf_op args[14]
  4.0 1.6 %copy.23.decay_w_ref = bf16[1024,2]{1,0:T(8,128)(2,1)} copy(bf16[1024,2]{0,1:T(2,128)(2,1)} %param.28) | data formatting | bytes 8192 | tf_op args[6]
  5.5 1.6 %copy.24.beta_w_ref = bf16[1024,2]{1,0:T(8,128)(2,1)} copy(bf16[1024,2]{0,1:T(2,128)(2,1)} %param.29) | data formatting | bytes 8192 | tf_op args[7]
  7.1 35.0 %layer_step.1 = bf16[16,256]{1,0:T(8,128)(2,1)} custom-call(bf16[16,1024]{1,0:T(8,128)(2,1)} %hidden_ref.1, f32[1,1024]{1,0:T(1,128)} %bitcast.4, bf16[1024,2]{1,0:T(8,128)(2,1)} %copy.23.decay_w_ref, bf16[1024,2]{1,0:T(8,128)(2,1)} %copy.24.beta_w_ref, f32[2]{0:T(128)} %decay_rate_ref.1, f32[1,128]{1,0:T(1,128)} %bitcast.6, f32[1,1024]{1,0:T(1,128)} %bitcast.5, ...), custom_call_target="tpu_custom_call" | custom-call | tf_op jit(solution)/shard_map/layer_step/pallas_call | solution.py:429
  42.1 1.3 %copy.28 = bf16[16,256]{1,0:T(8,128)(2,1)} copy(bf16[16,256]{1,0:T(8,128)(2,1)} %layer_step.1) | data formatting | bytes 16384

commit v2 on v1

--- a/solution.py
+++ b/solution.py
@@ -21,6 +21,10 @@
 
 def mm(lhs, rhs):
     return jnp.dot(lhs, rhs, preferred_element_type=jnp.float32)
+
+
+def mm_nt(lhs, rhs):
+    return lax.dot_general(lhs, rhs, NT, preferred_element_type=jnp.float32)
 
 
 def each(low, high, body):
@@ -72,6 +76,7 @@
     part,
     resid_v,
     rows,
+    wts,
     esend,
     erecv,
     fsend,
@@ -83,6 +88,10 @@
     part_recv,
     rows_send,
     rows_recv,
+    half_send,
+    half_recv,
+    wts_send,
+    wts_recv,
     e_send,
     e_recv,
     f_send,
@@ -163,7 +172,8 @@
     wide_all = ({}, {})
 
     def send_own(which):
-        src = (dgate_hbm, dup_hbm)[which]
+        src = wide.at[which, me_t]
+        wide_loads[which].wait()
         for bit in bits:
             copy = wide_copy(which, src, me_t, bit, bit)
             copy.start()
@@ -189,29 +199,42 @@
                         copy.start()
                         wide_all[which][mask + lower] = copy
 
-    send_own(0)
 
     hidden = hidden_ref[...].astype(jnp.float32)
     normed = rms_scale(hidden, mix_gain_ref[...], 0.1).astype(jnp.bfloat16)
-    beta = jax.nn.sigmoid(mm(normed, beta_w_ref[...]))
-    decay_pre = mm(normed, decay_w_ref[...])
+    beta = jax.nn.sigmoid(mm_nt(normed, beta_w_ref[...]))
+    decay_pre = mm_nt(normed, decay_w_ref[...])
     softplus = jnp.maximum(decay_pre, 0.0) + jnp.log1p(jnp.exp(-jnp.abs(decay_pre)))
-    group_row = group_ref[...]
     diagonal = lax.broadcasted_iota(jnp.int32, (seq, seq), 0) == lax.broadcasted_iota(
         jnp.int32, (seq, seq), 1
     )
-    group_col = jnp.sum(
-        jnp.where(diagonal, jnp.broadcast_to(group_row, (seq, seq)), 0.0), axis=1, keepdims=True
-    )
+
+    def column(row):
+        spread_row = jnp.broadcast_to(row, (seq, seq))
+        return jnp.sum(jnp.where(diagonal, spread_row, jnp.zeros_like(spread_row)), axis=1, keepdims=True)
+
     share = share_ref[...]
     ids = ids_ref[...]
-    route = group_col * share / jnp.sum(share, axis=1, keepdims=True)
-    pad = rows.shape[2] - width
+    route = group_ref[...] * share / jnp.sum(share, axis=0, keepdims=True)
+    pad = wts.shape[2]
     lanes = lax.broadcasted_iota(jnp.int32, (seq, pad), 1)
     spread = jnp.zeros((seq, pad), jnp.float32)
-    for k in range(ids.shape[1]):
-        spread = spread + jnp.where(ids[:, k : k + 1] == lanes, route[:, k : k + 1], 0.0)
-
+    for k in range(ids.shape[0]):
+        spread = spread + jnp.where(column(ids[k : k + 1]) == lanes, column(route[k : k + 1]), 0.0)
+
+    wts[me_e] = spread
+
+    def send_weights(step):
+        pltpu.make_async_remote_copy(
+            src_ref=wts.at[me_e],
+            dst_ref=wts.at[me_e],
+            send_sem=wts_send,
+            recv_sem=wts_recv,
+            device_id={"ep": (me_e + step) % n_ep},
+            device_id_type=MESH,
+        ).start()
+
+    each(1, n_ep, send_weights)
     for copy in qkv_loads:
         copy.wait()
     queries = mm(normed, qkv_v[0])
@@ -255,6 +278,7 @@
         )
         copy.start()
         part_copies.append(copy)
+    send_own(0)
     send_own(1)
     for copy in part_copies:
         copy.wait_recv()
@@ -263,13 +287,17 @@
         mix = mix + part[t].astype(jnp.float32)
     resid = (hidden + mix).astype(jnp.bfloat16).astype(jnp.float32)
     resid_v[...] = resid
-    rows[me_e, :, :width] = rms_scale(resid, ffn_gain_ref[...], 0.1).astype(jnp.bfloat16)
-    rows[me_e, :, width:] = spread.astype(jnp.bfloat16)
+    normed2 = rms_scale(resid, ffn_gain_ref[...], 0.1)
+    half = me_t % 2
+    half_width = width // 2
+    rows[half, me_e] = jnp.where(
+        half == 0, normed2[:, :half_width], normed2[:, half_width:]
+    ).astype(jnp.bfloat16)
 
     def send_rows(step):
         pltpu.make_async_remote_copy(
-            src_ref=rows.at[me_e],
-            dst_ref=rows.at[me_e],
+            src_ref=rows.at[half, me_e],
+            dst_ref=rows.at[half, me_e],
             send_sem=rows_send,
             recv_sem=rows_recv,
             device_id={"ep": (me_e + step) % n_ep},
@@ -284,15 +312,31 @@
     def wait_bytes(ref, sem):
         pltpu.make_async_copy(ref, ref, sem).wait()
 
-    wait_bytes(rows.at[pl.ds(0, n_ep - 1)], rows_recv)
+    wait_bytes(rows.at[half, pl.ds(0, n_ep - 1)], rows_recv)
+    half_copy = pltpu.make_async_remote_copy(
+        src_ref=rows.at[half],
+        dst_ref=rows.at[half],
+        send_sem=half_send,
+        recv_sem=half_recv,
+        device_id={"tp": partner(1)},
+        device_id_type=MESH,
+    )
+    half_copy.start()
+    wait_bytes(wts.at[pl.ds(0, n_ep - 1)], wts_recv)
+    half_copy.wait_recv()
 
     group = min(n_ep, 8)
     tall = group * seq
 
+    def token_rows(block):
+        at = pl.ds(block * group, group)
+        return jnp.concatenate(
+            [rows[side, at].reshape(tall, half_width) for side in (0, 1)], axis=1
+        )
+
     def expert_block(block):
-        both = rows[pl.ds(block * group, group)].reshape(tall, rows.shape[2])
-        row_block = both[:, :width]
-        weights = both[:, width:].astype(jnp.float32)
+        row_block = token_rows(block)
+        weights = wts[pl.ds(block * group, group)].reshape(tall, wts.shape[2])
         mine = lax.broadcasted_iota(jnp.int32, weights.shape, 1) == me_e
         weight = jnp.sum(jnp.where(mine, weights, 0.0), axis=1, keepdims=True)
         gate = mm(row_block, egu_v[0])
@@ -318,33 +362,36 @@
         )
         copy.start()
         e_copies.append(copy)
-    relay(1)
-    for copy in wide_loads:
-        copy.wait()
     down_load.wait()
-    last = [mask for mask in range(1, n_tp) if mask % 2 == 1]
-    for which in (0, 1):
-        for mask in last:
+
+    def wait_wide(which):
+        for mask in range(1, n_tp, 2):
             wide_all[which][mask].wait_recv()
 
-    def branch_block(block):
-        at = pl.ds(block * tall, tall)
-        row_block = rows[pl.ds(block * group, group)].reshape(tall, rows.shape[2])[:, :width]
-        gate, up = 0.0, 0.0
+    def term(row_block, which):
+        total = 0.0
         for t in range(n_tp):
             piece = row_block[:, t * quarter : (t + 1) * quarter]
-            gate = gate + lax.dot_general(
-                piece, wide[0, t], NT, preferred_element_type=jnp.float32
+            total = total + lax.dot_general(
+                piece, wide[which, t], NT, preferred_element_type=jnp.float32
             )
-            up = up + lax.dot_general(piece, wide[1, t], NT, preferred_element_type=jnp.float32)
-        unit = (gate * jax.nn.sigmoid(gate) * up).astype(jnp.bfloat16)
+        return total
+
+    def branch_weight(row_block):
+        products = 0.0
+        lane = branch_gate_ref.shape[1]
+        for c in range(branch_gate_ref.shape[0]):
+            piece = row_block[:, c * lane : (c + 1) * lane].astype(jnp.float32)
+            products = products + piece * branch_gate_ref[c : c + 1].astype(jnp.float32)
+        return jax.nn.sigmoid(jnp.sum(products, axis=1, keepdims=True))
+
+    def branch_block(block, row_block, gate, scale):
+        at = pl.ds(block * tall, tall)
+        gate = gate * jax.nn.sigmoid(gate)
+        up = term(row_block, 1)
+        unit = (gate * up).astype(jnp.bfloat16)
         branch = mm(unit, ddown_v[...])
-        pre = jnp.sum(
-            row_block.astype(jnp.float32) * branch_gate_ref[...].astype(jnp.float32),
-            axis=1,
-            keepdims=True,
-        )
-        return jax.nn.sigmoid(pre) * branch + esend[me_t, at].astype(jnp.float32)
+        return scale * branch + esend[me_t, at].astype(jnp.float32)
 
     def store_block(block, total):
         fsend[pl.ds(block * group, group)] = total.astype(jnp.bfloat16).reshape(
@@ -357,15 +404,29 @@
             total = total + erecv[step, at].astype(jnp.float32)
         store_block(block, total)
 
+    wait_wide(0)
     if n_ep == group:
-        total = branch_block(0)
+        row_block = token_rows(0)
+        gate = term(row_block, 0)
+        scale = branch_weight(row_block)
+        relay(1)
+        wait_wide(1)
+        total = branch_block(0, row_block, gate, scale)
         for copy in e_copies:
             copy.wait_recv()
         finish(0, total)
     else:
+        relay(1)
+        wait_wide(1)
         for copy in e_copies:
             copy.wait_recv()
-        each(0, n_ep // group, lambda block: finish(block, branch_block(block)))
+
+        def whole_block(block):
+            row_block = token_rows(block)
+            scale = branch_weight(row_block)
+            finish(block, branch_block(block, row_block, term(row_block, 0), scale))
+
+        each(0, n_ep // group, whole_block)
 
     def send_final(step):
         peer = (me_e + step) % n_ep
@@ -385,7 +446,9 @@
     total = total + jnp.sum(frecv[...].astype(jnp.float32), axis=0)
     out_ref[...] = total.astype(jnp.bfloat16)
     wait_bytes(frecv, f_send)
-    wait_bytes(rows.at[pl.ds(0, n_ep - 1)], rows_send)
+    wait_bytes(rows.at[half, pl.ds(0, n_ep - 1)], rows_send)
+    wait_bytes(wts.at[pl.ds(0, n_ep - 1)], wts_send)
+    half_copy.wait_send()
     for copy in part_copies + e_copies:
         copy.wait_send()
     for which in (0, 1):
@@ -444,7 +507,8 @@
             pltpu.VMEM((2, n_tp) + dense_gate.shape, bf16),
             pltpu.VMEM((n_tp, seq, width), bf16),
             pltpu.VMEM((seq, width), jnp.float32),
-            pltpu.VMEM((n_ep, seq, width + pad), bf16),
+            pltpu.VMEM((2, n_ep, seq, width // 2), bf16),
+            pltpu.VMEM((n_ep, seq, pad), jnp.float32),
             pltpu.VMEM((n_tp, tokens, quarter), bf16),
             pltpu.VMEM((n_tp - 1, tokens, quarter), bf16),
             pltpu.VMEM((n_ep, seq, quarter), bf16),
@@ -456,6 +520,10 @@
             dma((n_tp,)),
             dma,
             dma,
+            dma,
+            dma,
+            dma,
+            dma,
             dma((n_tp,)),
             dma((n_tp,)),
             dma,
@@ -468,15 +536,15 @@
     )(
         hidden_in,
         mix_gain[None, :],
-        decay_w,
-        beta_w,
+        decay_w.T,
+        beta_w.T,
         decay_rate,
         head_gain[None, :],
         ffn_gain[None, :],
-        expert_ids,
+        expert_ids.T,
         group_share[None, :],
-        expert_share,
-        branch_gate[None, :],
+        expert_share.T,
+        branch_gate.reshape(width // 128, 128),
         prior_state,
         query_w,
         key_w,

time: 43.8 us -> 31 us (0.71)
  local copies, waits for them, and re-layouts: 8.39 us -> 1.3 us
  Pallas kernels: 35 us -> 29.4 us
    unnamed x5 -> x1, local copies, waits for them, and re-layouts: 7.11 us -> 1.3 us
    pallas_call x1, Pallas kernels: 35 us -> 29.4 us  [local(): pl.pallas_call(functools.partial(kernel, n_ep, n_tp), out_shape=jax.Shape...]
    broadcast_in_dim x1 -> x0, local copies, waits for them, and re-layouts: 1.28 us -> none  [local(): branch_gate[None, :]]
where the time goes in v2:
time: 31 us; the launch traced here: 30.7 us
  Pallas kernels  29.4 us (95%)
  local copies, waits for them, and re-layouts  1.3 us (4%)
    pallas_call x1, Pallas kernels, local(): pl.pallas_call(functools.partial(kernel, n_ep, n_tp), out_shape=jax.Shape...  29.4 us
    unnamed x1, local copies, waits for them, and re-layouts  1.3 us

profile of v2, /device:TPU:0, one launch (start us, length us, event | category | flops | bytes accessed | tf_op | source)
XLA Modules:
  0.0 30.7 jit_solution(2603148427009083272)
XLA Ops:
  0.0 29.4 %layer_step.1 = bf16[16,256]{1,0:T(8,128)(2,1)} custom-call(bf16[16,1024]{1,0:T(8,128)(2,1)} %hidden_ref.1, f32[1,1024]{1,0:T(1,128)} %bitcast.9, bf16[2,1024]{1,0:T(2,128)(2,1)} %bitcast.10, bf16[2,1024]{1,0:T(2,128)(2,1)} %bitcast.11, f32[2]{0:T(128)} %decay_rate_ref.1, f32[1,128]{1,0:T(1,128)} %bitcast.16, f32[1,1024]{1,0:T(1,128)} %bitcast.12, ...), custom_call_target="tpu_custom_call" | custom-call | tf_op jit(solution)/shard_map/layer_step/pallas_call | solution.py:492
  29.4 1.3 %copy.24 = bf16[16,256]{1,0:T(8,128)(2,1)} copy(bf16[16,256]{1,0:T(8,128)(2,1)} %layer_step.1) | data formatting | bytes 16384
